TPU v7x, 32 devices: a whole 2x2x4 slice. The times are simulated.
32 devices in a mesh: sp: 16 (over z, y, x), tp: 2 (over core).
Axes of the slice: x: 2, y: 2, z: 4, core: 2. Of those that a mesh axis runs over, the one named last changes fastest.
Arguments:
- tokens: bfloat16 [4096, 2048], P('sp'), as said below
- in_gain: float32 [2048], replicated, may hold values from 0.1 to 1.9
- w_query: bfloat16 [2048, 1024], P(None, 'tp'), as said below
- w_key: bfloat16 [2048, 1024], P(None, 'tp'), may hold values from -0.125 to 0.125
- w_value: bfloat16 [2048, 1024], P(None, 'tp'), may hold values from -0.125 to 0.125
- lam: float32 [8], P('tp'), may hold values from 0.3 to 0.8
- sub_gain: float32 [128], replicated, may hold values from 0.1 to 1.9
- w_out: bfloat16 [1024, 2048], P('tp'), may hold values from -0.1875 to 0.1875
Outputs:
- mixed: bfloat16 [4096, 2048], P('sp')
Inputs may be any that keep to these rules, and one draw needn't show every extreme that they name: tokens: normal entries plus, for each block of 64 tokens, a factor times one direction common to all tokens. w_query: independent normal entries.
All inputs are finite; a program needn't handle non-finite values.
Results may differ from a plain program's by a relative error of at most 0.025.
The roundings to bfloat16 on the way count: a program that leaves them out, or rounds other values in their place, can miss the bound.
Values may be sent and summed in bfloat16 or wider, within the bound.
A program may use at most 64 MiB of HBM per device.

v0:
```python
import jax
import jax.numpy as jnp
from jax import lax
from jax.sharding import PartitionSpec as P

KD = 64
VD = 128


def rotate(vectors, position):
    half = vectors.shape[-1] // 2
    freq = 500000.0 ** (-jnp.arange(0, 2 * half, 2, dtype=jnp.float32) / (2 * half))
    angle = position.astype(jnp.float32)[:, None] * freq[None, :]
    cosine = jnp.cos(angle)[:, None, :]
    sine = jnp.sin(angle)[:, None, :]
    first = vectors[..., :half]
    second = vectors[..., half:]
    return jnp.concatenate(
        [first * cosine - second * sine, second * cosine + first * sine], axis=-1
    )


def shards(tokens, in_gain, w_query, w_key, w_value, lam, sub_gain, w_out):
    span = tokens.shape[0]
    local_heads = lam.shape[0]
    xfloat = tokens.astype(jnp.float32)
    normed = (
        xfloat * lax.rsqrt(jnp.mean(xfloat * xfloat, axis=-1, keepdims=True) + 1e-06) * in_gain
    ).astype(jnp.bfloat16)
    weights_all = jnp.concatenate([w_query, w_key, w_value], axis=1)
    projected = jnp.dot(normed, weights_all, preferred_element_type=jnp.float32)
    qcols = local_heads * 2 * KD
    position = lax.axis_index("sp") * span + jnp.arange(span, dtype=jnp.int32)
    queries = rotate(projected[:, :qcols].reshape(span, 2 * local_heads, KD), position).astype(
        jnp.bfloat16
    )
    queries = queries.reshape(span, local_heads, 2, KD)
    keys = rotate(
        projected[:, qcols : 2 * qcols].reshape(span, 2 * local_heads, KD), position
    ).astype(jnp.bfloat16)
    keys = keys.reshape(span, qcols)
    values = projected[:, 2 * qcols :].astype(jnp.bfloat16)
    scale = KD ** (-0.5)

    def update(carry, key_piece, value_piece):
        top, mass, accum = carry
        count = key_piece.shape[0]
        key_four = key_piece.reshape(count, local_heads, 2, KD)
        value_three = value_piece.reshape(count, local_heads, VD)
        scores = (
            jnp.einsum("qhcd,khcd->hcqk", queries, key_four, preferred_element_type=jnp.float32)
            * scale
        )
        new_top = jnp.maximum(top, jnp.max(scores, axis=-1))
        factor = jnp.exp(top - new_top)
        expo = jnp.exp(scores - new_top[..., None])
        mass = mass * factor + jnp.sum(expo, axis=-1)
        weights = expo.astype(jnp.bfloat16)
        accum = accum * factor[..., None] + jnp.einsum(
            "hcqk,khe->hcqe", weights, value_three, preferred_element_type=jnp.float32
        )
        return (new_top, mass, accum)

    start_carry = (
        jnp.full((local_heads, 2, span), -1e30, jnp.float32),
        jnp.zeros((local_heads, 2, span), jnp.float32),
        jnp.zeros((local_heads, 2, span, VD), jnp.float32),
    )
    carry = start_carry
    key_piece = lax.all_gather(keys, "sp", axis=0, tiled=True)
    value_piece = lax.all_gather(values, "sp", axis=0, tiled=True)
    count = key_piece.shape[0]

    def step_block(inner, items):
        return (update(inner, items[0], items[1]), None)

    blocks = (
        key_piece.reshape(count // 512, 512, key_piece.shape[1]),
        value_piece.reshape(count // 512, 512, value_piece.shape[1]),
    )
    carry, unused = lax.scan(step_block, carry, blocks)
    top, mass, accum = carry
    read = accum / mass[..., None]
    diff = read[:, 0] - lam[:, None, None] * read[:, 1]
    normal = diff * lax.rsqrt(jnp.mean(diff * diff, axis=-1, keepdims=True) + 1e-05) * sub_gain
    attended = jnp.transpose(normal, (1, 0, 2)).reshape(span, local_heads * VD).astype(jnp.bfloat16)
    share = lax.psum_scatter(
        jnp.dot(attended, w_out, preferred_element_type=jnp.float32).astype(jnp.bfloat16),
        "tp",
        scatter_dimension=0,
        tiled=True,
    )
    result = lax.all_gather(share, "tp", axis=0, tiled=True)
    return result


def solution(mesh):
    in_specs = (
        P("sp", None),
        P(),
        P(None, "tp"),
        P(None, "tp"),
        P(None, "tp"),
        P("tp"),
        P(),
        P("tp", None),
    )
    out_specs = P("sp", None)
    return jax.shard_map(shards, mesh=mesh, in_specs=in_specs, out_specs=out_specs, check_vma=False)
```

profile of v0, /device:TPU:1, one launch (start us, length us, event | category | flops | bytes accessed | tf_op | source)
XLA Modules:
  0.0 281.0 jit_solution(3731221670889648921)
XLA Ops:
  6.6 1.7 fusion.19
  8.2 5.0 %fusion.13 = f32[256,1536]{1,0:T(8,128)S(1)} fusion(bf16[2048,512]{1,0:T(8,128)(2,1)} %param.14, bf16[2048,512]{1,0:T(8,128)(2,1)} %param.13, bf16[2048,512]{1,0:T(8,128)(2,1)} %param.12, bf16[256,2048]{1,0:T(8,128)(2,1)} %param.10, f32[2048]{0:T(1024)} %param.11, f32[256]{0:T(256)S(1)} %add_rsqrt_fusion.1), kind=kOutput, calls=%fused_computation.18 | convolution fusion | flops 1631584256 | bytes 8922112 | tf_op jit(solution)/shard_map/dot_general | solution.py:31
  13.3 1.0 fusion.28
  14.8 1.2 copy.15
  16.4 0.7 pad_maximum_fusion
  17.2 1.8 slice.71
  19.2 85.5 %all-gather.4.cloned.1.call-done = bf16[4096,512]{0,1:T(8,128)(2,1)} async-done(((bf16[256,512]{0,1:T(8,128)(2,1)}), bf16[4096,512]{0,1:T(8,128)(2,1)}) %all-gather.4.cloned.1.call-update) | async-done | bytes 4194320 | tf_op jit(solution)/shard_map/all_gather | solution.py:70
  104.7 6.5 %copy.16 = bf16[4096,512]{1,0:T(8,128)(2,1)} copy(bf16[4096,512]{0,1:T(8,128)(2,1)} %all-gather.4.cloned.1.call-done) | data formatting | bytes 8388608 | tf_op jit(solution)/shard_map/all_gather | solution.py:70
  111.2 70.0 %all-gather.6.cloned.1.call-done = bf16[4096,512]{1,0:T(8,128)(2,1)} async-done(((bf16[256,512]{1,0:T(8,128)(2,1)}), bf16[4096,512]{1,0:T(8,128)(2,1)}) %all-gather.6.cloned.1.call-update) | async-done | bytes 4194320 | tf_op jit(solution)/shard_map/all_gather | solution.py:71
  181.1 66.4 %while.15 = (s32[]{:T(128)}, f32[4,2,256]{2,1,0:T(2,128)S(1)}, f32[4,2,256]{2,1,0:T(2,128)S(1)}, f32[4,2,256,128]{3,2,1,0:T(8,128)}, bf16[8,512,512]{2,1,0:T(8,1...) while((s32[]{:T(128)}, f32[4,2,256]{2,1,0:T(2,128)S(1)}, ...), condition=%wide.region_4.5_spmd.clone, body=%wide.region_1.4_spmd.clone.sunk | while | flops 411838464 | bytes 30802120 | solution.py:81
  181.1 2.1 constant_dynamic-slice_fusion.3
  183.2 1.3 copy.30
  184.5 1.0 copy.31
  185.5 0.8 bitcast_reduce_fusion.2
  187.1 1.4 fusion.49
  188.5 0.9 copy-done.3
  189.4 2.1 constant_dynamic-slice_fusion.3
  191.5 1.3 copy.30
  192.8 1.0 copy.31
  193.8 0.8 bitcast_reduce_fusion.2
  195.4 1.4 fusion.49
  196.8 0.9 copy-done.3
  197.7 2.1 constant_dynamic-slice_fusion.3
  199.8 1.3 copy.30
  201.1 1.0 copy.31
  202.1 0.8 bitcast_reduce_fusion.2
  203.7 1.4 fusion.49
  205.1 0.9 copy-done.3
  206.0 2.1 constant_dynamic-slice_fusion.3
  208.1 1.3 copy.30
  209.4 1.0 copy.31
  210.4 0.8 bitcast_reduce_fusion.2
  212.0 1.4 fusion.49
  213.4 0.9 copy-done.3
  214.3 2.1 constant_dynamic-slice_fusion.3
  216.4 1.3 copy.30
  217.7 1.0 copy.31
  218.7 0.8 bitcast_reduce_fusion.2
  219.5 0.7 fusion.47
  220.3 1.4 fusion.49
  221.7 0.9 copy-done.3
  222.6 2.1 constant_dynamic-slice_fusion.3
  224.7 1.3 copy.30
  226.0 1.0 copy.31
  227.0 0.8 bitcast_reduce_fusion.2
  228.6 1.4 fusion.49
  230.0 0.9 copy-done.3
  230.9 2.1 constant_dynamic-slice_fusion.3
  233.0 1.3 copy.30
  234.3 1.0 copy.31
  235.3 0.8 bitcast_reduce_fusion.2
  236.9 1.4 fusion.49
  238.3 0.9 copy-done.3
  239.2 2.1 constant_dynamic-slice_fusion.3
  241.3 1.3 copy.30
  242.6 1.0 copy.31
  243.6 0.8 bitcast_reduce_fusion.2
  245.2 1.4 fusion.49
  246.6 0.9 copy-done.3
  247.6 1.6 copy.21
  249.6 1.7 convolution_convert_fusion
  251.4 9.2 %reduce-scatter.2.cloned.1.call-done = bf16[128,2048]{1,0:T(8,128)(2,1)} async-done(((bf16[256,2048]{1,0:T(8,128)(2,1)}), bf16[128,2048]{1,0:T(8,128)(2,1)}) %reduce-scatter.2.cloned.1.call-update) | async-done | bytes 524304 | tf_op jit(solution)/shard_map/reduce_scatter | solution.py:87
  260.6 11.6 %all-gather.8.cloned.1.call-done = bf16[256,2048]{1,0:T(8,128)(2,1)} async-done(((bf16[128,2048]{1,0:T(8,128)(2,1)}), bf16[256,2048]{1,0:T(8,128)(2,1)}) %all-gather.8.cloned.1.call-update) | async-done | bytes 1048592 | tf_op jit(solution)/shard_map/all_gather | solution.py:93
  272.2 2.3 copy.45
  (102 shorter events, 6.9 us)
Async XLA Ops:
  6.5 243.1 %copy-start = (bf16[512,2048]{1,0:T(8,128)(2,1)S(1)}, bf16[512,2048]{1,0:T(8,128)(2,1)}, u32[]{:S(2)}) copy-start(bf16[512,2048]{1,0:T(8,128)(2,1)} %param.17) | copy-start | bytes 6291460
  6.5 98.1 %all-gather.4.cloned.1.call-start = ((), (), s32[]{:S(2)}) async-start(), calls=%async_computation.1 | async-start | bytes 4456448 | tf_op jit(solution)/shard_map/all_gather | solution.py:70
  13.3 1.4 copy-start.4
  17.2 163.9 %all-gather.6.cloned.1.call-start = ((), (), s32[]{:S(2)}) async-start(), calls=%async_computation.2 | async-start | bytes 4456448 | tf_op jit(solution)/shard_map/all_gather | solution.py:71
  19.1 241.5 %reduce-scatter.2.cloned.1.call-start = ((), (), s32[]{:S(2)}) async-start(), calls=%async_computation.3 | async-start | bytes 1572864 | tf_op jit(solution)/shard_map/reduce_scatter | solution.py:87
  185.5 1.5 copy-start.1
  185.5 1.5 copy-start.2
  188.5 1.0 copy-start.3
  193.8 1.5 copy-start.1
  193.8 1.5 copy-start.2
  196.8 1.0 copy-start.3
  202.1 1.5 copy-start.1
  202.1 1.5 copy-start.2
  205.1 1.0 copy-start.3
  210.4 1.5 copy-start.1
  210.4 1.5 copy-start.2
  213.4 1.0 copy-start.3
  218.7 1.5 copy-start.1
  218.7 1.5 copy-start.2
  221.7 1.0 copy-start.3
  227.0 1.5 copy-start.1
  227.0 1.5 copy-start.2
  230.0 1.0 copy-start.3
  235.3 1.5 copy-start.1
  235.3 1.5 copy-start.2
  238.3 1.0 copy-start.3
  243.6 1.5 copy-start.1
  243.6 1.5 copy-start.2
  246.6 1.0 copy-start.3
  247.6 1.7 copy-start.5
  247.6 1.9 copy-start.6
  251.3 20.9 %all-gather.8.cloned.1.call-start = ((), (), s32[]{:S(2)}) async-start(), calls=%async_computation.4 | async-start | bytes 1572864 | tf_op jit(solution)/shard_map/all_gather | solution.py:93
Sparse Core Ops, SparseCore 0:
  17.3 87.3 all-gather.3
  107.4 73.6 all-gather.5
  251.5 9.0 reduce-scatter.1
  262.0 10.1 all-gather.7
where the time goes:
time: 282 us; the launch traced here: 281 us
  waiting for transfers between devices  176 us (62%)
  local copies, waits for them, and re-layouts  57.7 us (20%)
  matrix products  24 us (9%)
  between operations  13.3 us (5%)
  other arithmetic  9.1 us (3%)
    all_gather x1, waiting for transfers between devices, shards(): key_piece = lax.all_gather(keys, 'sp', axis=0, tiled=True)  85.5 us
    all_gather x1, waiting for transfers between devices, shards(): value_piece = lax.all_gather(values, 'sp', axis=0, tiled=True)  70 us
    dynamic_slice x24, local copies, waits for them, and re-layouts, shards(): carry, unused = lax.scan(step_block, carry, blocks)  35 us
    all_gather x1, waiting for transfers between devices, shards(): result = lax.all_gather(share, 'tp', axis=0, tiled=True)  11.6 us
    dot_general x8, matrix products, update(): jnp.einsum('hcqk,khe->hcqe', weights, value_three, preferred_element_type...  11.1 us
    reduce_scatter x1, waiting for transfers between devices, shards(): lax.psum_scatter(jnp.dot(attended, w_out, preferred_element_type=jnp.floa...  9.17 us
    while x56, local copies, waits for them, and re-layouts  7.71 us
    all_gather x1, local copies, waits for them, and re-layouts, shards(): key_piece = lax.all_gather(keys, 'sp', axis=0, tiled=True)  6.49 us
  transfers between devices with their start and end apart: 4, of which 4 were waited for; matrix products, arithmetic and copies ran while one was open for 3% of the time, Pallas kernels for 0%

commit v1 on v0

v1 whole, which is shorter than its diff:
```python
import functools

import jax
import jax.numpy as jnp
from jax import lax
from jax.experimental import pallas as pl
from jax.experimental.pallas import tpu as pltpu
from jax.sharding import PartitionSpec as P

KD = 64
VD = 128
HW = 2 * KD
MESH = pl.DeviceIdType.MESH
LOG2E = 1.4426950408889634


def kernel(
    dims,
    tok_hbm,
    gain_ref,
    wq_hbm,
    wk_hbm,
    wv_hbm,
    lam_ref,
    sub_ref,
    wo_hbm,
    cos_ref,
    sin_ref,
    out_ref,
    tok,
    wq,
    wk,
    wv,
    wo,
    normed,
    qst,
    kst,
    vst,
    qbuf,
    kbuf,
    vbuf,
    acc,
    top,
    mass,
    attst,
    att,
    load_sem,
    send_sem,
    q_sem,
    k_sem,
    v_sem,
    a_sem,
    w_sem,
):
    H, R, TP, span = dims
    sp = lax.axis_index("sp")
    tpi = lax.axis_index("tp")
    g = sp // R
    r = sp % R
    sent = []

    def head_peer(d):
        return (g + d) % H

    def row_peer(d):
        if R == 4:
            x, y = r % 2, r // 2
            return [None, y * 2 + (1 - x), (1 - y) * 2 + x, 3 - r][d]
        return (r + d) % R

    def at(group, row):
        return {"sp": group * R + row}

    def remote(src, dst, recv, device):
        copy = pltpu.make_async_remote_copy(
            src_ref=src,
            dst_ref=dst,
            send_sem=send_sem.at[len(sent)],
            recv_sem=recv,
            device_id=device,
            device_id_type=MESH,
        )
        copy.start()
        sent.append(copy)

    def arrived(dst, recv):
        pltpu.make_async_remote_copy(
            src_ref=dst,
            dst_ref=dst,
            send_sem=send_sem.at[0],
            recv_sem=recv,
            device_id={"tp": (tpi + 1) % TP},
            device_id_type=MESH,
        ).wait_recv()

    loads = [
        pltpu.make_async_copy(tok_hbm, tok, load_sem.at[0]),
        pltpu.make_async_copy(wq_hbm, wq, load_sem.at[1]),
        pltpu.make_async_copy(wk_hbm, wk, load_sem.at[2]),
        pltpu.make_async_copy(wv_hbm, wv, load_sem.at[3]),
        pltpu.make_async_copy(
            wo_hbm, wo.at[pl.ds(pl.multiple_of(tpi * (H * VD), VD), H * VD)], load_sem.at[4]
        ),
    ]
    for load in loads[:4]:
        load.start()

    barrier = pltpu.get_barrier_semaphore()
    for d in range(1, H):
        pl.semaphore_signal(barrier, inc=1, device_id=at(head_peer(d), r), device_id_type=MESH)
    for d in range(1, R):
        pl.semaphore_signal(barrier, inc=1, device_id=at(g, row_peer(d)), device_id_type=MESH)
    for d in range(1, TP):
        pl.semaphore_signal(barrier, inc=1, device_id={"tp": (tpi + d) % TP}, device_id_type=MESH)

    loads[0].wait()
    rows = 32

    def norm_rows(i, carry):
        part = pl.ds(pl.multiple_of(i * rows, rows), rows)
        x = tok[part, :].astype(jnp.float32)
        mean = jnp.mean(x * x, axis=-1, keepdims=True)
        normed[part, :] = (x * lax.rsqrt(mean + 1e-06) * gain_ref[...]).astype(jnp.bfloat16)
        return carry

    lax.fori_loop(0, span // rows, norm_rows, 0)

    lane = lax.broadcasted_iota(jnp.int32, (span, HW), 1)
    low = (lane % KD) < (KD // 2)

    def rotated(x):
        other = jnp.where(low, pltpu.roll(x, HW - KD // 2, 1), pltpu.roll(x, KD // 2, 1))
        return (x * cos_ref[...] + other * sin_ref[...]).astype(jnp.bfloat16)

    def project(weight, stage, turn):
        y = jnp.dot(normed[...], weight[...], preferred_element_type=jnp.float32)
        for h in range(H):
            z = y[:, h * HW : (h + 1) * HW]
            stage[h] = rotated(z) if turn else z.astype(jnp.bfloat16)

    loads[1].wait()
    project(wq, qst, True)
    pl.semaphore_wait(barrier, (H - 1) + (R - 1) + (TP - 1))
    for d in range(1, H):
        to = head_peer(d)
        remote(qst.at[to], qbuf.at[g], q_sem.at[g], at(to, r))
    qbuf[g] = qst[g]
    for weight, stage, buf, sem, load in (
        (wk, kst, kbuf, k_sem, loads[2]),
        (wv, vst, vbuf, v_sem, loads[3]),
    ):
        load.wait()
        project(weight, stage, stage is kst)
        for d in range(1, H):
            to = head_peer(d)
            remote(stage.at[to], buf.at[g, r], sem.at[g, r], at(to, r))
        buf[g, r] = stage[g]
        for d in range(1, R):
            remote(stage.at[g], buf.at[g, r], sem.at[g, r], at(g, row_peer(d)))
    own_rows = pl.ds(pl.multiple_of(tpi * (H * VD), VD), H * VD)
    loads[4].start()
    for d in range(1, TP):
        remote(wo_hbm, wo.at[own_rows], w_sem.at[tpi], {"tp": (tpi + d) % TP})

    def spread(s):
        gs = head_peer(s)
        for buf, sem in ((kbuf, k_sem), (vbuf, v_sem)):
            arrived(buf.at[gs, r], sem.at[gs, r])
            for d in range(1, R):
                remote(buf.at[gs, r], buf.at[gs, r], sem.at[gs, r], at(g, row_peer(d)))

    RC = max(1, min(R, 1024 // span))
    while R % RC:
        RC -= 1
    nu = R // RC
    keys = RC * span
    scale = LOG2E * KD ** (-0.5)

    def attend(gs, u, t, first):
        kb = kbuf[gs, pl.ds(u * RC, RC)].reshape(keys, HW)
        vb = vbuf[gs, pl.ds(u * RC, RC)].reshape(keys, VD)
        q = qbuf[t]
        for c in range(2):
            qc = jnp.where((lane // KD) == c, q, jnp.zeros_like(q))
            s = lax.dot_general(
                qc, kb, (((1,), (1,)), ((), ())), preferred_element_type=jnp.float32
            )
            new = jnp.max(s, axis=-1, keepdims=True) * scale
            if not first:
                old = top[t, c][:, :1]
                new = jnp.maximum(new, old)
            p = jnp.exp2(s * scale - new)
            total = jnp.sum(p, axis=-1, keepdims=True)
            read = jnp.dot(p.astype(jnp.bfloat16), vb, preferred_element_type=jnp.float32)
            if first:
                acc[t, c] = read
                mass[t, c] = jnp.broadcast_to(total, (span, VD))
            else:
                factor = jnp.exp2(old - new)
                acc[t, c] = acc[t, c] * factor + read
                mass[t, c] = mass[t, c] * factor + total
            top[t, c] = jnp.broadcast_to(new, (span, VD))

    def finish(t):
        diff = acc[t, 0] / mass[t, 0] - lam_ref[g] * (acc[t, 1] / mass[t, 1])
        mean = jnp.mean(diff * diff, axis=-1, keepdims=True)
        return (diff * lax.rsqrt(mean + 1e-05) * sub_ref[...]).astype(jnp.bfloat16)

    def column(tp, h):
        return pl.ds(pl.multiple_of((tp * H + h) * VD, VD), VD)

    for d in range(1, H):
        arrived(qbuf.at[head_peer(d)], q_sem.at[head_peer(d)])

    if nu > 1:
        top[...] = jnp.full(top.shape, -1e30, jnp.float32)
        mass[...] = jnp.zeros(mass.shape, jnp.float32)
        acc[...] = jnp.zeros(acc.shape, jnp.float32)

    def finish_and_send(j):
        t = (g + 1 + j) % H
        done = finish(t)
        if j == H - 1:
            att[:, column(tpi, g)] = done
        else:
            attst[j] = done
            remote(attst.at[j], att.at[:, column(tpi, g)], a_sem.at[tpi * H + g], at(t, r))

    for s in range(H):
        gs = head_peer(s)
        if s + 1 < H:
            spread(s + 1)
        for d in range(1, R):
            rs = row_peer(d)
            arrived(kbuf.at[gs, rs], k_sem.at[gs, rs])
            arrived(vbuf.at[gs, rs], v_sem.at[gs, rs])
        if nu > 1:

            def chunk(i, carry):
                attend(gs, i // H, i % H, False)
                return carry

            lax.fori_loop(0, nu * H, chunk, 0)
        elif s < H - 1:

            def tile(t, carry):
                attend(gs, 0, t, s == 0)
                return carry

            lax.fori_loop(0, H, tile, 0)
        else:
            for j in range(H):
                attend(gs, 0, (g + 1 + j) % H, s == 0)
                finish_and_send(j)
    if nu > 1:
        for j in range(H):
            finish_and_send(j)

    def pass_on(h):
        for d in range(1, TP):
            remote(
                att.at[:, column(tpi, h)],
                att.at[:, column(tpi, h)],
                a_sem.at[tpi * H + h],
                {"tp": (tpi + d) % TP},
            )

    pass_on(g)
    for d in range(H - 1, 0, -1):
        h = head_peer(d)
        arrived(att.at[:, column(tpi, h)], a_sem.at[tpi * H + h])
        pass_on(h)
    loads[4].wait()
    for d in range(1, TP):
        other = (tpi + d) % TP
        arrived(wo.at[pl.ds(pl.multiple_of(other * (H * VD), VD), H * VD)], w_sem.at[other])
        for h in range(H):
            arrived(att.at[:, column(other, h)], a_sem.at[other * H + h])

    width = min(512, out_ref.shape[1])
    for n in range(out_ref.shape[1] // width):
        part = slice(n * width, (n + 1) * width)
        out_ref[:, part] = jnp.dot(
            att[...], wo[:, part], preferred_element_type=jnp.float32
        ).astype(out_ref.dtype)
    for copy in sent:
        copy.wait_send()


def shards(sp_size, tp_size, tokens, in_gain, w_query, w_key, w_value, lam, sub_gain, w_out):
    span, model = tokens.shape
    H = lam.shape[0]
    R = sp_size // H
    TP = tp_size
    half = KD // 2
    freq = 500000.0 ** (-jnp.arange(0, 2 * half, 2, dtype=jnp.float32) / (2 * half))
    position = lax.axis_index("sp") * span + jnp.arange(span, dtype=jnp.int32)
    angle = position.astype(jnp.float32)[:, None] * freq[None, :]
    cosine = jnp.cos(angle)
    sine = jnp.sin(angle)
    cosine = jnp.concatenate([cosine] * 4, axis=1)
    sine = jnp.concatenate([-sine, sine] * 2, axis=1)
    bf16, f32 = jnp.bfloat16, jnp.float32
    sends = 3 * (H - 1) + 2 * H * (R - 1) + (TP - 1) + (H - 1) + H * (TP - 1)
    hbm = pl.BlockSpec(memory_space=pl.ANY)
    vmem = pl.BlockSpec(memory_space=pltpu.VMEM)
    smem = pl.BlockSpec(memory_space=pltpu.SMEM)
    DMA = pltpu.SemaphoreType.DMA
    return pl.pallas_call(
        functools.partial(kernel, (H, R, TP, span)),
        out_shape=jax.ShapeDtypeStruct((span, model), bf16),
        in_specs=[hbm, vmem, hbm, hbm, hbm, smem, vmem, hbm, vmem, vmem],
        out_specs=vmem,
        scratch_shapes=[
            pltpu.VMEM(tokens.shape, bf16),
            pltpu.VMEM(w_query.shape, bf16),
            pltpu.VMEM(w_key.shape, bf16),
            pltpu.VMEM(w_value.shape, bf16),
            pltpu.VMEM((TP * H * VD, model), bf16),
            pltpu.VMEM(tokens.shape, bf16),
            pltpu.VMEM((H, span, HW), bf16),
            pltpu.VMEM((H, span, HW), bf16),
            pltpu.VMEM((H, span, VD), bf16),
            pltpu.VMEM((H, span, HW), bf16),
            pltpu.VMEM((H, R, span, HW), bf16),
            pltpu.VMEM((H, R, span, VD), bf16),
            pltpu.VMEM((H, 2, span, VD), f32),
            pltpu.VMEM((H, 2, span, VD), f32),
            pltpu.VMEM((H, 2, span, VD), f32),
            pltpu.VMEM((max(1, H - 1), span, VD), bf16),
            pltpu.VMEM((span, TP * H * VD), bf16),
            DMA((5,)),
            DMA((sends,)),
            DMA((H,)),
            DMA((H, R)),
            DMA((H, R)),
            DMA((TP * H,)),
            DMA((TP,)),
        ],
        compiler_params=pltpu.CompilerParams(
            collective_id=0, has_side_effects=True, vmem_limit_bytes=60 * 1024 * 1024
        ),
        name="layer",
    )(
        tokens,
        in_gain.reshape(1, -1),
        w_query,
        w_key,
        w_value,
        lam,
        sub_gain.reshape(1, -1),
        w_out,
        cosine,
        sine,
    )


def solution(mesh):
    in_specs = (
        P("sp", None),
        P(),
        P(None, "tp"),
        P(None, "tp"),
        P(None, "tp"),
        P("tp"),
        P(),
        P("tp", None),
    )
    out_specs = P("sp", None)
    body = functools.partial(shards, mesh.shape["sp"], mesh.shape["tp"])
    return jax.shard_map(body, mesh=mesh, in_specs=in_specs, out_specs=out_specs, check_vma=False)
```

time: 282 us -> 59.2 us (0.21)
  waiting for transfers between devices: 176 us -> 0 us
  local copies, waits for them, and re-layouts: 57.7 us -> 2.3 us
  Pallas kernels: 0 us -> 55.1 us
  matrix products: 24 us -> 0 us
  between operations: 13.3 us -> 0.02 us
  other arithmetic: 9.1 us -> 1.52 us
    all_gather x3 -> x0, waiting for transfers between devices: 167 us -> none  [the longest x1 85.5 us: shards(): key_piece = lax.all_gather(keys, 'sp', axis=0, tiled=True)]
    pallas_call x0 -> x1, Pallas kernels: none -> 55.1 us  [shards(): pl.pallas_call(functools.partial(kernel, (H, R, TP, span)), out_shape=jax...]
    dynamic_slice x24 -> x0, local copies, waits for them, and re-layouts: 35 us -> none  [shards(): carry, unused = lax.scan(step_block, carry, blocks)]
    dot_general x18 -> x0, matrix products: 24 us -> none  [the longest x8 11.1 us: update(): jnp.einsum('hcqk,khe->hcqe', weights, value_three, preferred_element_type...]
    while x58 -> x0, local copies, waits for them, and re-layouts: 9.29 us -> none
    reduce_scatter x1 -> x0, waiting for transfers between devices: 9.17 us -> none  [shards(): lax.psum_scatter(jnp.dot(attended, w_out, preferred_element_type=jnp.floa...]
    reduce_sum x10 -> x0, other arithmetic: 7.44 us -> none  [the longest x8 5.63 us: update(): mass = mass * factor + jnp.sum(expo, axis=-1)]
    all_gather x1 -> x0, local copies, waits for them, and re-layouts: 6.49 us -> none  [shards(): key_piece = lax.all_gather(keys, 'sp', axis=0, tiled=True)]
  transfers between devices with their start and end apart: 4 -> 0, of which waited for: 4 -> 0; matrix products, arithmetic and copies ran while one was open for 3% -> 0% of each run, Pallas kernels for 0% -> 0%
where the time goes in v1:
time: 59.2 us; the launch traced here: 59 us
  Pallas kernels  55.1 us (93%)
  local copies, waits for them, and re-layouts  2.3 us (4%)
  other arithmetic  1.52 us (3%)
    pallas_call x1, Pallas kernels, shards(): pl.pallas_call(functools.partial(kernel, (H, R, TP, span)), out_shape=jax...  55.1 us
    unnamed x1, local copies, waits for them, and re-layouts  2.3 us

profile of v1, /device:TPU:1, one launch (start us, length us, event | category | flops | bytes accessed | tf_op | source)
XLA Modules:
  0.0 59.0 jit_solution(13394900488411905406)
XLA Ops:
  0.0 0.5 fusion
  0.6 1.0 %pad_maximum_fusion = (f32[256,128]{1,0:T(8,128)}, f32[256,128]{1,0:T(8,128)}) fusion(f32[256,32]{1,0:T(8,128)S(1)} %get-tuple-element.7, f32[256,32]{1,0:T(8,128)S(1)} %get-tuple-element.6, f32[256,32]{1,0:T(8,128)S(1)} %get-tuple-element.5), kind=kLoop, calls=%fused_computation.2 | loop fusion | flops 196608 | bytes 360448 | tf_op jit(solution)/shard_map/concatenate | solution.py:301
  1.5 55.1 %layer.1 = bf16[256,2048]{1,0:T(8,128)(2,1)} custom-call(bf16[256,2048]{1,0:T(8,128)(2,1)} %tok_hbm.1, f32[1,2048]{1,0:T(1,128)} %bitcast.2, bf16[2048,512]{1,0:T(8,128)(2,1)} %wq_hbm.1, bf16[2048,512]{1,0:T(8,128)(2,1)} %wk_hbm.1, bf16[2048,512]{1,0:T(8,128)(2,1)} %wv_hbm.1, f32[4]{0:T(128)} %lam_ref.1, f32[1,128]{1,0:T(1,128)} %bitcast.3, ...), custom_call_target="tpu_custom_call" | custom-call | tf_op jit(solution)/shard_map/layer/pallas_call | solution.py:309
  56.7 2.3 %copy.11 = bf16[256,2048]{1,0:T(8,128)(2,1)} copy(bf16[256,2048]{1,0:T(8,128)(2,1)} %layer.1) | data formatting | bytes 2097152
  (2 shorter events, 0.0 us)

commit v2 on v1

--- a/solution.py
+++ b/solution.py
@@ -151,7 +151,7 @@
     ):
         load.wait()
         project(weight, stage, stage is kst)
-        for d in range(1, H):
+        for d in range(H - 1, 0, -1):
             to = head_peer(d)
             remote(stage.at[to], buf.at[g, r], sem.at[g, r], at(to, r))
         buf[g, r] = stage[g]

time: 59.2 us -> 58 us (0.980)
  Pallas kernels: 55.1 us -> 54 us
    pallas_call x1, Pallas kernels: 55.1 us -> 54 us  [shards(): pl.pallas_call(functools.partial(kernel, (H, R, TP, span)), out_shape=jax...]
where the time goes in v2:
time: 58 us; the launch traced here: 57.8 us
  Pallas kernels  54 us (93%)
  local copies, waits for them, and re-layouts  2.3 us (4%)
  other arithmetic  1.52 us (3%)
    pallas_call x1, Pallas kernels, shards(): pl.pallas_call(functools.partial(kernel, (H, R, TP, span)), out_shape=jax...  54 us
    unnamed x1, local copies, waits for them, and re-layouts  2.3 us

profile of v2, /device:TPU:1, one launch (start us, length us, event | category | flops | bytes accessed | tf_op | source)
XLA Modules:
  0.0 57.8 jit_solution(16878467339198411271)
XLA Ops:
  0.0 0.5 fusion
  0.6 1.0 %pad_maximum_fusion = (f32[256,128]{1,0:T(8,128)}, f32[256,128]{1,0:T(8,128)}) fusion(f32[256,32]{1,0:T(8,128)S(1)} %get-tuple-element.7, f32[256,32]{1,0:T(8,128)S(1)} %get-tuple-element.6, f32[256,32]{1,0:T(8,128)S(1)} %get-tuple-element.5), kind=kLoop, calls=%fused_computation.2 | loop fusion | flops 196608 | bytes 360448 | tf_op jit(solution)/shard_map/concatenate | solution.py:301
  1.5 54.0 %layer.1 = bf16[256,2048]{1,0:T(8,128)(2,1)} custom-call(bf16[256,2048]{1,0:T(8,128)(2,1)} %tok_hbm.1, f32[1,2048]{1,0:T(1,128)} %bitcast.2, bf16[2048,512]{1,0:T(8,128)(2,1)} %wq_hbm.1, bf16[2048,512]{1,0:T(8,128)(2,1)} %wk_hbm.1, bf16[2048,512]{1,0:T(8,128)(2,1)} %wv_hbm.1, f32[4]{0:T(128)} %lam_ref.1, f32[1,128]{1,0:T(1,128)} %bitcast.3, ...), custom_call_target="tpu_custom_call" | custom-call | tf_op jit(solution)/shard_map/layer/pallas_call | solution.py:309
  55.5 2.3 %copy.11 = bf16[256,2048]{1,0:T(8,128)(2,1)} copy(bf16[256,2048]{1,0:T(8,128)(2,1)} %layer.1) | data formatting | bytes 2097152
  (2 shorter events, 0.0 us)
